TPU v7x, 128 devices: a whole 4x4x4 slice. The times are simulated.
128 devices in a mesh: sp: 32 (over z, y, core), tp: 4 (over x).
Axes of the slice: x: 4, y: 4, z: 4, core: 2. Of those that a mesh axis runs over, the one named last changes fastest.
Arguments:
- residual_in: bfloat16 [65536, 2048], P(('sp', 'tp')), may hold values from -6 to 6
- conv_input: bfloat16 [65536, 1024], P('sp', 'tp'), may hold values from -6 to 6
- input_gate: bfloat16 [65536, 1024], P('sp', 'tp'), may hold values from -6 to 6
- output_gate: bfloat16 [65536, 1024], P('sp', 'tp'), may hold values from -6 to 6
- conv_taps: bfloat16 [3, 1024], P(None, 'tp'), may hold values from -3.5 to 3.5
- doc_ids: int32 [65536], P('sp'), may hold values from 0 to 15, never falling along the last dimension, each value on 1 to 8192 neighbouring positions
- proj_weight: bfloat16 [1024, 2048], replicated, may hold values from -0.1875 to 0.1875
- norm_gain: float32 [2048], replicated, may hold values from 0.1 to 1.9
- expert_ids: int32 [65536, 2], P(('sp', 'tp')), may hold values from 0 to 31, all different within a row; in each aligned block of 512 rows (0 to 511, 512 to 1023, ...) at most 64 rows name the same one
- expert_weight: float32 [65536, 2], P(('sp', 'tp')), may hold values from 0.05 to 1
- w_gate: bfloat16 [32, 2048, 512], P('sp'), may hold values from -0.125 to 0.125
- w_up: bfloat16 [32, 2048, 512], P('sp'), may hold values from -0.125 to 0.125
- w_down: bfloat16 [32, 512, 2048], P('sp'), may hold values from -0.25 to 0.25
Outputs:
- layer_out: bfloat16 [65536, 2048], P(('sp', 'tp'))
Inputs may be any that keep to these rules, and one draw needn't show every extreme that they name: `doc_ids`: numbers never fall along the sequence; one document spans at most 8192 positions. `expert_ids`: a token's two experts differ; in each aligned block of rows that one device holds, no expert is named more than 64 times, a bound that some block reaches.
All inputs are finite; a program needn't handle non-finite values.
Results may differ from a plain program's by a relative error of at most 0.0047.
Values may be sent and summed in bfloat16 or wider, within the bound.
A program may use at most 128 MiB of HBM per device.

v0:
```python
import jax
import jax.numpy as jnp
from jax import lax
from jax.sharding import PartitionSpec as P

EXPERTS = 32
CAP = 64
epsilon = 1e-06
F32 = jnp.float32
BF16 = jnp.bfloat16


def from_behind(x, axis, by):
    devices = lax.axis_size(axis)
    pairs = [(i, i + by) for i in range(devices) if 0 <= i + by < devices]
    return lax.ppermute(x, axis, pairs)


def per_device(
    residual_in,
    conv_input,
    input_gate,
    output_gate,
    conv_taps,
    doc_ids,
    proj_weight,
    norm_gain,
    expert_ids,
    expert_weight,
    w_gate,
    w_up,
    w_down,
):
    kernel_width = conv_taps.shape[0]
    rim = kernel_width - 1
    length, channels = conv_input.shape
    doc_float = doc_ids.astype(F32)
    tail = input_gate[-rim:].astype(F32) * conv_input[-rim:].astype(F32)
    packed = jnp.concatenate([tail, jnp.broadcast_to(doc_float[-rim:, None], (rim, 128))], axis=1)
    prev = from_behind(packed, "sp", 1)
    prev_in, prev_ids = (prev[:, :channels], prev[:, channels])
    first = lax.axis_index("sp") == 0
    prev_ids = jnp.where(first, -1.0, prev_ids)
    product = input_gate.astype(F32) * conv_input.astype(F32)
    padded_in = jnp.concatenate([prev_in, product], axis=0)
    padded_ids = jnp.concatenate([prev_ids, doc_float], axis=0)
    conv_sum = jnp.zeros(product.shape, F32)
    for offset in range(kernel_width):
        same_doc = padded_ids[offset : offset + length] == doc_float
        term = conv_taps[offset].astype(F32)[None, :] * padded_in[offset : offset + length]
        conv_sum = conv_sum + jnp.where(same_doc[:, None], term, 0.0)
    gated = (output_gate.astype(F32) * conv_sum).astype(BF16)
    regrouped = lax.all_to_all(gated, "tp", split_axis=0, concat_axis=1, tiled=True)
    tokens = expert_ids.shape[0]
    experts = jnp.arange(EXPERTS, dtype=jnp.int32)
    ids_t = expert_ids.T
    weight_t = expert_weight.T
    hit = [ids_t[j][None, :] == experts[:, None] for j in range(2)]
    used = hit[0] | hit[1]
    weight_of = jnp.where(hit[0], weight_t[0][None, :], 0.0) + jnp.where(
        hit[1], weight_t[1][None, :], 0.0
    )
    t_row = lax.broadcasted_iota(jnp.int32, (tokens, tokens), 0)
    t_col = lax.broadcasted_iota(jnp.int32, (tokens, tokens), 1)
    earlier = (t_row < t_col).astype(BF16)
    rank = jnp.dot(used.astype(BF16), earlier, preferred_element_type=F32)
    code = jnp.where(used, rank, -1.0)
    slot_of = lax.broadcasted_iota(jnp.int32, (EXPERTS, CAP, tokens), 1).astype(F32)
    match = code[:, None, :] == slot_of
    dispatch = match.astype(BF16).reshape(EXPERTS * CAP, tokens)
    combine = (
        jnp.where(match, weight_of[:, None, :], 0.0).astype(BF16).reshape(EXPERTS * CAP, tokens)
    )
    mixed = jnp.dot(regrouped, proj_weight, preferred_element_type=F32)
    hidden = residual_in.astype(F32) + mixed
    scale_rows = lax.rsqrt(jnp.mean(hidden * hidden, axis=-1, keepdims=True) + epsilon)
    normed = (hidden * scale_rows * norm_gain[None, :]).astype(BF16)
    width = normed.shape[1]
    buffer = jnp.dot(dispatch, normed, preferred_element_type=F32).astype(BF16)
    buffer = buffer.reshape(EXPERTS, CAP, width)
    slots = lax.all_to_all(buffer, "sp", split_axis=0, concat_axis=0, tiled=True).reshape(
        EXPERTS * CAP, width
    )
    gate_val = jnp.dot(slots, w_gate[0], preferred_element_type=F32)
    up_val = jnp.dot(slots, w_up[0], preferred_element_type=F32)
    act_rows = (jax.nn.silu(gate_val) * up_val).astype(BF16)
    expert_out = jnp.dot(act_rows, w_down[0], preferred_element_type=F32).astype(BF16)
    expert_out = expert_out.reshape(EXPERTS, CAP, width)
    returned = lax.all_to_all(expert_out, "sp", split_axis=0, concat_axis=0, tiled=True).reshape(
        EXPERTS * CAP, width
    )
    expert_sum = lax.dot_general(
        combine, returned, (((0,), (0,)), ((), ())), preferred_element_type=F32
    )
    return (hidden + expert_sum).astype(BF16)


def solution(mesh):
    return jax.shard_map(
        per_device,
        mesh=mesh,
        in_specs=(
            P(("sp", "tp"), None),
            P("sp", "tp"),
            P("sp", "tp"),
            P("sp", "tp"),
            P(None, "tp"),
            P("sp"),
            P(),
            P(),
            P(("sp", "tp"), None),
            P(("sp", "tp"), None),
            P("sp", None, None),
            P("sp", None, None),
            P("sp", None, None),
        ),
        out_specs=P(("sp", "tp"), None),
        check_vma=False,
    )
```

profile of v0, /device:TPU:0, one launch (start us, length us, event | category | flops | bytes accessed | tf_op | source)
XLA Modules:
  0.0 288.9 jit_solution(236948942608263788)
XLA Ops:
  0.0 0.8 convert_element_type.61
  0.9 0.1 slice.64
  0.9 0.7 convert_multiply_fusion.1
  1.7 1.4 collective-permute-start
  3.2 3.1 %convert_multiply_fusion = f32[2048,256]{1,0:T(8,128)} fusion(bf16[2048,256]{1,0:T(8,128)(2,1)} %param.14, bf16[2048,256]{1,0:T(8,128)(2,1)} %param.15), kind=kLoop, calls=%fused_computation.31 | loop fusion | flops 1572864 | bytes 4194304 | tf_op jit(solution)/shard_map/mul | solution.py:44
  6.3 0.1 fusion.27
  6.4 0.1 fusion.25
  6.5 5.9 %fusion.7 = bf16[2048,256]{1,0:T(8,128)(2,1)} fusion(f32[2,256]{1,0:T(2,128)S(1)} %slice.68, f32[2048,256]{1,0:T(8,128)} %convert_multiply_fusion, bf16[2048,256]{1,0:T(8,128)(2,1)S(1)} %copy-done.4, f32[256]{0:T(256)S(1)} %bitcast.51, f32[256]{0:T(256)S(1)} %bitcast.52, f32[256]{0:T(256)S(1)} %bitcast.50, pred[2048]{0:T(1024)(128)(4,1)S(1)} %convert_compare_fusion, ...), kind=kLoop, calls=%fused_computation.18 | loop fusion | flops 6815744 | bytes 4205568 | tf_op jit(solution)/shard_map/convert_element_type | solution.py:52
  12.4 5.0 %all-to-all-start = ((bf16[4,512,256]{2,1,0:T(8,128)(2,1)}), bf16[4,512,256]{2,1,0:T(8,128)(2,1)S(1)}, u32[]{:S(2)}, u32[]{:S(2)}) async-start(bf16[4,512,256]{2,1,0:T(8,128)(2,1)} %bitcast.43), calls=%async_computation | async-start | bytes 2097152 | tf_op jit(solution)/shard_map/all_to_all | solution.py:53
  17.4 0.1 iota.41
  17.5 0.2 convolution_select_fusion
  17.7 1.6 bitcast_compare_fusion
  19.3 14.0 %all-to-all-done = bf16[4,512,256]{2,1,0:T(8,128)(2,1)S(1)} async-done(((bf16[4,512,256]{2,1,0:T(8,128)(2,1)}), bf16[4,512,256]{2,1,0:T(8,128)(2,1)S(1)}, u32[]{:S(2)}, u32[]{:S(2)}) %all-to-all-start) | async-done | bytes 1048608 | tf_op jit(solution)/shard_map/all_to_all | solution.py:53
  33.3 1.0 copy-done.2
  34.3 1.5 copy.15
  35.8 5.8 %multiply_reduce_fusion = (f32[512]{0:T(512)S(1)}, f32[512,2048]{1,0:T(8,128)S(1)}) fusion(bf16[512,1024]{0,1:T(8,128)(2,1)S(1)} %bitcast.41, bf16[1024,2048]{1,0:T(8,128)(2,1)} %param.19, bf16[512,2048]{1,0:T(8,128)(2,1)} %param.13), kind=kOutput, calls=%fused_computation.7 | convolution fusion | flops 2151677440 | bytes 11536384 | tf_op jit(solution)/shard_map/dot_general | solution.py:74
  41.6 5.1 %convolution_convert_fusion.1 = bf16[2048,2048]{1,0:T(8,128)(2,1)S(1)} fusion(pred[2048,512]{1,0:T(32,128)(4,1)S(1)} %copy-done.3, f32[512,2048]{1,0:T(8,128)S(1)} %get-tuple-element.15, f32[2048]{0:T(1024)S(1)} %copy-done.11, f32[512]{0:T(512)S(1)} %add_rsqrt_fusion), kind=kOutput, calls=%fused_computation.1 | convolution fusion | flops 4302307328 | bytes 13641728 | tf_op jit(solution)/shard_map/dot_general | solution.py:79
  46.7 104.8 %all_to_all.29 = bf16[32,64,2048]{2,1,0:T(8,128)(2,1)S(1)} all-to-all(bf16[32,64,2048]{2,1,0:T(8,128)(2,1)S(1)} %bitcast.38), channel_id=1, replica_groups=mesh['sp'=32,'tp'=4] {'sp'}, dimensions={0} | all-to-all | bytes 16777216 | tf_op jit(solution)/shard_map/all_to_all | solution.py:81
  151.5 4.5 %fusion.12 = f32[2048,512]{1,0:T(8,128)S(1)} fusion(bf16[2048,2048]{1,0:T(8,128)(2,1)S(1)} %bitcast.39, bf16[1,2048,512]{2,1,0:T(8,128)(2,1)S(1)} %copy-done.9), kind=kOutput, calls=%fused_computation.24 | convolution fusion | flops 4294967296 | bytes 14680064 | tf_op jit(solution)/shard_map/dot_general | solution.py:84
  156.1 5.2 %multiply_convert_fusion = bf16[2048,512]{1,0:T(8,128)(2,1)S(1)} fusion(f32[2048,512]{1,0:T(8,128)S(1)} %fusion.12, bf16[2048,2048]{1,0:T(8,128)(2,1)S(1)} %bitcast.40, bf16[1,2048,512]{2,1,0:T(8,128)(2,1)S(1)} %copy-done.10), kind=kOutput, calls=%fused_computation.5 | convolution fusion | flops 4301258752 | bytes 16777216 | tf_op jit(solution)/shard_map/dot_general | solution.py:85
  161.2 6.7 %convolution_convert_fusion = bf16[2048,2048]{1,0:T(8,128)(2,1)} fusion(bf16[2048,512]{1,0:T(8,128)(2,1)S(1)} %multiply_convert_fusion, bf16[1,512,2048]{2,1,0:T(8,128)(2,1)S(1)} %copy-done), kind=kOutput, calls=%fused_computation | convolution fusion | flops 4299161600 | bytes 12582912 | tf_op jit(solution)/shard_map/dot_general | solution.py:87
  168.0 5.1 %all-to-all-start.2 = ((bf16[32,64,2048]{2,1,0:T(8,128)(2,1)}), bf16[32,64,2048]{2,1,0:T(8,128)(2,1)}, u32[]{:S(2)}, u32[]{:S(2)}) async-start(bf16[32,64,2048]{2,1,0:T(8,128)(2,1)} %bitcast.37), calls=%async_computation.2 | async-start | bytes 16777216 | tf_op jit(solution)/shard_map/all_to_all | solution.py:89
  173.1 105.8 %all-to-all-done.2 = bf16[32,64,2048]{2,1,0:T(8,128)(2,1)} async-done(((bf16[32,64,2048]{2,1,0:T(8,128)(2,1)}), bf16[32,64,2048]{2,1,0:T(8,128)(2,1)}, u32[]{:S(2)}, u32[]{:S(2)}) %all-to-all-start.2) | async-done | bytes 8388640 | tf_op jit(solution)/shard_map/all_to_all | solution.py:89
  279.0 9.9 %fusion = bf16[512,2048]{1,0:T(8,128)(2,1)} fusion(f32[512,2048]{1,0:T(8,128)} %copy-done.1, bf16[32,64,2048]{2,1,0:T(8,128)(2,1)} %all-to-all-done.2, bf16[32,512]{1,0:T(8,128)(2,1)S(1)} %select_add_fusion, f32[32,512]{1,0:T(8,128)S(1)} %convolution_select_fusion, f32[64]{0:T(128)S(1)} %iota_convert_fusion), kind=kOutput, calls=%fused_computation.3 | convolution fusion | flops 4299161600 | bytes 14778624 | tf_op jit(solution)/shard_map/dot_general | solution.py:92
  (35 shorter events, 0.2 us)
Async XLA Ops:
  0.0 161.2 %copy-start = (bf16[1,512,2048]{2,1,0:T(8,128)(2,1)S(1)}, bf16[1,512,2048]{2,1,0:T(8,128)(2,1)}, u32[]{:S(2)}) copy-start(bf16[1,512,2048]{2,1,0:T(8,128)(2,1)} %param.25) | copy-start | bytes 6291460
  0.9 5.4 %copy-start.5 = (s32[2048]{0:T(1024)S(1)}, s32[2048]{0:T(1024)}, u32[]{:S(2)}) copy-start(s32[2048]{0:T(1024)} %param.18) | copy-start | bytes 24580
  1.7 4.5 %copy-start.6 = (bf16[3,256]{1,0:T(4,128)(2,1)S(1)}, bf16[3,256]{1,0:T(4,128)(2,1)}, u32[]{:S(2)}) copy-start(bf16[3,256]{1,0:T(4,128)(2,1)} %param.17) | copy-start | bytes 4612
  1.7 4.8 %copy-start.4 = (bf16[2048,256]{1,0:T(8,128)(2,1)S(1)}, bf16[2048,256]{1,0:T(8,128)(2,1)}, u32[]{:S(2)}) copy-start(bf16[2048,256]{1,0:T(8,128)(2,1)} %param.16) | copy-start | bytes 3145732
  1.7 4.6 %collective-permute-start = (f32[2,384]{1,0:T(2,128)S(1)}, f32[2,384]{1,0:T(2,128)S(1)}, u32[]{:S(2)}, u32[]{:S(2)}) collective-permute-start(f32[2,384]{1,0:T(2,128)S(1)} %pad_maximum_fusion.2), channel_id=1, source_target_pairs={{0,4},{4,8},{8,12},{12,16},{16,20},{20,24},{24,28},{28,32},{32,36}... | collective-permute-start | bytes 9224 | tf_op jit(solution)/shard_map/ppermute | solution.py:16
  12.4 5.1 %copy-start.7 = (s32[512,2]{0,1:T(2,128)S(1)}, s32[512,2]{0,1:T(2,128)}, u32[]{:S(2)}) copy-start(s32[512,2]{0,1:T(2,128)} %param.21) | copy-start | bytes 12292
  12.4 20.9 %all-to-all-start = ((bf16[4,512,256]{2,1,0:T(8,128)(2,1)}), bf16[4,512,256]{2,1,0:T(8,128)(2,1)S(1)}, u32[]{:S(2)}, u32[]{:S(2)}) async-start(bf16[4,512,256]{2,1,0:T(8,128)(2,1)} %bitcast.43), calls=%async_computation | async-start | bytes 2097152 | tf_op jit(solution)/shard_map/all_to_all | solution.py:53
  33.3 1.0 copy-start.2
  35.8 5.8 %copy-start.3 = (pred[2048,512]{1,0:T(32,128)(4,1)S(1)}, pred[2048,512]{1,0:T(32,128)(4,1)}, u32[]{:S(2)}) copy-start(pred[2048,512]{1,0:T(32,128)(4,1)} %bitcast_compare_fusion) | copy-start | bytes 3145732
  35.8 5.8 %copy-start.11 = (f32[2048]{0:T(1024)S(1)}, f32[2048]{0:T(1024)}, u32[]{:S(2)}) copy-start(f32[2048]{0:T(1024)} %param.20) | copy-start | bytes 24580
  41.6 5.1 %copy-start.1 = (f32[512,2048]{1,0:T(8,128)}, f32[512,2048]{1,0:T(8,128)S(1)}, u32[]{:S(2)}) copy-start(f32[512,2048]{1,0:T(8,128)S(1)} %get-tuple-element.15) | copy-start | bytes 12582916
  46.7 104.8 %copy-start.9 = (bf16[1,2048,512]{2,1,0:T(8,128)(2,1)S(1)}, bf16[1,2048,512]{2,1,0:T(8,128)(2,1)}, u32[]{:S(2)}) copy-start(bf16[1,2048,512]{2,1,0:T(8,128)(2,1)} %param.23) | copy-start | bytes 6291460
  151.5 4.5 %copy-start.10 = (bf16[1,2048,512]{2,1,0:T(8,128)(2,1)S(1)}, bf16[1,2048,512]{2,1,0:T(8,128)(2,1)}, u32[]{:S(2)}) copy-start(bf16[1,2048,512]{2,1,0:T(8,128)(2,1)} %param.24) | copy-start | bytes 6291460
  168.0 5.1 %copy-start.8 = (f32[512,2]{0,1:T(2,128)S(1)}, f32[512,2]{0,1:T(2,128)}, u32[]{:S(2)}) copy-start(f32[512,2]{0,1:T(2,128)} %param.22) | copy-start | bytes 12292
  168.0 111.0 %all-to-all-start.2 = ((bf16[32,64,2048]{2,1,0:T(8,128)(2,1)}), bf16[32,64,2048]{2,1,0:T(8,128)(2,1)}, u32[]{:S(2)}, u32[]{:S(2)}) async-start(bf16[32,64,2048]{2,1,0:T(8,128)(2,1)} %bitcast.37), calls=%async_computation.2 | async-start | bytes 16777216 | tf_op jit(solution)/shard_map/all_to_all | solution.py:89
where the time goes:
time: 289 us
  waiting for transfers between devices  120 us (42%)
  blocking collectives  105 us (36%)
  matrix products  37.4 us (13%)
  other arithmetic  12.4 us (4%)
  starting transfers between devices  11.5 us (4%)
    all_to_all x1, waiting for transfers between devices, per_device(): lax.all_to_all(expert_out, 'sp', split_axis=0, concat_axis=0, tiled=True)  106 us
    all_to_all x1, blocking collectives, per_device(): lax.all_to_all(buffer, 'sp', split_axis=0, concat_axis=0, tiled=True)  105 us
    all_to_all x1, waiting for transfers between devices, per_device(): lax.all_to_all(gated, 'tp', split_axis=0, concat_axis=1, tiled=True)  14 us
    dot_general x1, matrix products, per_device(): lax.dot_general(combine, returned, (((0,), (0,)), ((), ())), preferred_el...  9.88 us
    dot_general x1, matrix products, per_device(): jnp.dot(act_rows, w_down[0], preferred_element_type=F32).astype(BF16)  6.74 us
    convert_element_type x1, other arithmetic, per_device(): gated = (output_gate.astype(F32) * conv_sum).astype(BF16)  5.9 us
    dot_general x1, matrix products, per_device(): mixed = jnp.dot(regrouped, proj_weight, preferred_element_type=F32)  5.8 us
  transfers between devices with their start and end apart: 3, of which 2 were waited for; matrix products, arithmetic and copies ran while one was open for 2% of the time, Pallas kernels for 0%

commit v1 on v0

--- a/solution.py
+++ b/solution.py
@@ -50,7 +50,9 @@
         term = conv_taps[offset].astype(F32)[None, :] * padded_in[offset : offset + length]
         conv_sum = conv_sum + jnp.where(same_doc[:, None], term, 0.0)
     gated = (output_gate.astype(F32) * conv_sum).astype(BF16)
-    regrouped = lax.all_to_all(gated, "tp", split_axis=0, concat_axis=1, tiled=True)
+    regrouped = jnp.concatenate(
+        lax.all_to_all(jnp.stack(jnp.split(gated, lax.axis_size("tp"), axis=0)), "tp", 0, 0), axis=1
+    )
     tokens = expert_ids.shape[0]
     experts = jnp.arange(EXPERTS, dtype=jnp.int32)
     ids_t = expert_ids.T

time: 289 us -> 292 us (1.010)
  local copies, waits for them, and re-layouts: 2.74 us -> 5.74 us
    unnamed x24 -> x25, local copies, waits for them, and re-layouts: 1.02 us -> 5.29 us
  transfers between devices with their start and end apart: 3 -> 3, of which waited for: 2 -> 2; matrix products, arithmetic and copies ran while one was open for 2% -> 4% of each run, Pallas kernels for 0% -> 0%
where the time goes in v1:
time: 292 us
  waiting for transfers between devices  120 us (41%)
  blocking collectives  105 us (36%)
  matrix products  37.3 us (13%)
  other arithmetic  12.9 us (4%)
  starting transfers between devices  11.2 us (4%)
  local copies, waits for them, and re-layouts  5.74 us (2%)
    all_to_all x1, waiting for transfers between devices, per_device(): lax.all_to_all(expert_out, 'sp', split_axis=0, concat_axis=0, tiled=True)  106 us
    all_to_all x1, blocking collectives, per_device(): lax.all_to_all(buffer, 'sp', split_axis=0, concat_axis=0, tiled=True)  105 us
    all_to_all x1, waiting for transfers between devices, per_device(): lax.all_to_all(jnp.stack(jnp.split(gated, lax.axis_size('tp'), axis=0)),...  14 us
    dot_general x1, matrix products, per_device(): lax.dot_general(combine, returned, (((0,), (0,)), ((), ())), preferred_el...  9.88 us
    dot_general x1, matrix products, per_device(): jnp.dot(act_rows, w_down[0], preferred_element_type=F32).astype(BF16)  6.71 us
  transfers between devices with their start and end apart: 3, of which 2 were waited for; matrix products, arithmetic and copies ran while one was open for 4% of the time, Pallas kernels for 0%

profile of v1, /device:TPU:0, one launch (start us, length us, event | category | flops | bytes accessed | tf_op | source)
XLA Modules:
  0.0 292.0 jit_solution(3263590335518976606)
XLA Ops:
  0.0 0.9 convert_element_type.61
  0.9 0.7 convert_multiply_fusion.1
  1.9 1.3 collective-permute-start
  3.2 1.5 copy.20
  4.7 2.3 copy.21
  7.0 0.6 convert_compare_fusion
  7.5 2.9 convert_multiply_fusion
  10.4 0.6 slice_convert_fusion.2
  11.0 1.5 copy.18
  12.7 4.4 %fusion.7 = bf16[2048,256]{0,1:T(8,128)(2,1)S(1)} fusion(f32[2,256]{0,1:T(8,128)S(1)} %slice.68, f32[2048,256]{0,1:T(8,128)} %convert_multiply_fusion, bf16[2048,256]{0,1:T(8,128)(2,1)S(1)} %copy.18, f32[256]{0:T(256)} %bitcast.59, f32[256]{0:T(256)} %bitcast.60, f32[256]{0:T(256)} %bitcast.58, pred[2048]{0:T(1024)(128)(4,1)S(1)} %copy-done.4, ...), kind=kLoop, calls=%fused_computation.18 | loop fusion | flops 6815744 | bytes 4205568 | tf_op jit(solution)/shard_map/convert_element_type | solution.py:52
  17.1 1.1 pad_maximum_fusion.1
  18.2 4.9 %all-to-all-start = ((bf16[4,512,256]{1,2,0:T(8,128)(2,1)}), bf16[4,512,256]{1,2,0:T(8,128)(2,1)S(1)}, u32[]{:S(2)}, u32[]{:S(2)}) async-start(bf16[4,512,256]{1,2,0:T(8,128)(2,1)} %pad_maximum_fusion.1), calls=%async_computation | async-start | bytes 2097152 | tf_op jit(solution)/shard_map/all_to_all | solution.py:54
  23.2 0.2 convolution_select_fusion
  23.4 1.6 bitcast_compare_fusion
  25.0 14.0 %all-to-all-done = bf16[4,512,256]{1,2,0:T(8,128)(2,1)S(1)} async-done(((bf16[4,512,256]{1,2,0:T(8,128)(2,1)}), bf16[4,512,256]{1,2,0:T(8,128)(2,1)S(1)}, u32[]{:S(2)}, u32[]{:S(2)}) %all-to-all-start) | async-done | bytes 1048608 | tf_op jit(solution)/shard_map/all_to_all | solution.py:54
  39.0 5.8 %multiply_reduce_fusion = (f32[512]{0:T(512)S(1)}, f32[512,2048]{1,0:T(8,128)S(1)}) fusion(bf16[512,1024]{0,1:T(8,128)(2,1)S(1)} %bitcast.51, bf16[1024,2048]{1,0:T(8,128)(2,1)} %param.19, bf16[512,2048]{1,0:T(8,128)(2,1)} %param.13), kind=kOutput, calls=%fused_computation.7 | convolution fusion | flops 2151677440 | bytes 11536384 | tf_op jit(solution)/shard_map/dot_general | solution.py:76
  44.8 5.1 %convolution_convert_fusion.1 = bf16[2048,2048]{1,0:T(8,128)(2,1)S(1)} fusion(pred[2048,512]{1,0:T(32,128)(4,1)S(1)} %copy-done.2, f32[512,2048]{1,0:T(8,128)S(1)} %get-tuple-element.19, f32[2048]{0:T(1024)S(1)} %copy-done.10, f32[512]{0:T(512)S(1)} %add_rsqrt_fusion), kind=kOutput, calls=%fused_computation.1 | convolution fusion | flops 4302307328 | bytes 13641728 | tf_op jit(solution)/shard_map/dot_general | solution.py:81
  50.0 104.8 %all_to_all.15 = bf16[32,64,2048]{2,1,0:T(8,128)(2,1)S(1)} all-to-all(bf16[32,64,2048]{2,1,0:T(8,128)(2,1)S(1)} %bitcast.48), channel_id=1, replica_groups=mesh['sp'=32,'tp'=4] {'sp'}, dimensions={0} | all-to-all | bytes 16777216 | tf_op jit(solution)/shard_map/all_to_all | solution.py:83
  154.7 4.5 %fusion.12 = f32[2048,512]{1,0:T(8,128)S(1)} fusion(bf16[2048,2048]{1,0:T(8,128)(2,1)S(1)} %bitcast.49, bf16[1,2048,512]{2,1,0:T(8,128)(2,1)S(1)} %copy-done.8), kind=kOutput, calls=%fused_computation.24 | convolution fusion | flops 4294967296 | bytes 14680064 | tf_op jit(solution)/shard_map/dot_general | solution.py:86
  159.3 5.2 %multiply_convert_fusion = bf16[2048,512]{1,0:T(8,128)(2,1)S(1)} fusion(f32[2048,512]{1,0:T(8,128)S(1)} %fusion.12, bf16[2048,2048]{1,0:T(8,128)(2,1)S(1)} %bitcast.50, bf16[1,2048,512]{2,1,0:T(8,128)(2,1)S(1)} %copy-done.9), kind=kOutput, calls=%fused_computation.5 | convolution fusion | flops 4301258752 | bytes 16777216 | tf_op jit(solution)/shard_map/dot_general | solution.py:87
  164.5 6.7 %convolution_convert_fusion = bf16[2048,2048]{1,0:T(8,128)(2,1)} fusion(bf16[2048,512]{1,0:T(8,128)(2,1)S(1)} %multiply_convert_fusion, bf16[1,512,2048]{2,1,0:T(8,128)(2,1)S(1)} %copy-done), kind=kOutput, calls=%fused_computation | convolution fusion | flops 4299161600 | bytes 12582912 | tf_op jit(solution)/shard_map/dot_general | solution.py:89
  171.2 5.1 %all-to-all-start.2 = ((bf16[32,64,2048]{2,1,0:T(8,128)(2,1)}), bf16[32,64,2048]{2,1,0:T(8,128)(2,1)}, u32[]{:S(2)}, u32[]{:S(2)}) async-start(bf16[32,64,2048]{2,1,0:T(8,128)(2,1)} %bitcast.47), calls=%async_computation.2 | async-start | bytes 16777216 | tf_op jit(solution)/shard_map/all_to_all | solution.py:91
  176.3 105.8 %all-to-all-done.2 = bf16[32,64,2048]{2,1,0:T(8,128)(2,1)} async-done(((bf16[32,64,2048]{2,1,0:T(8,128)(2,1)}), bf16[32,64,2048]{2,1,0:T(8,128)(2,1)}, u32[]{:S(2)}, u32[]{:S(2)}) %all-to-all-start.2) | async-done | bytes 8388640 | tf_op jit(solution)/shard_map/all_to_all | solution.py:91
  282.1 9.9 %fusion = bf16[512,2048]{1,0:T(8,128)(2,1)} fusion(f32[512,2048]{1,0:T(8,128)} %copy-done.1, bf16[32,64,2048]{2,1,0:T(8,128)(2,1)} %all-to-all-done.2, bf16[32,512]{1,0:T(8,128)(2,1)S(1)} %select_add_fusion, f32[32,512]{1,0:T(8,128)S(1)} %convolution_select_fusion, f32[64]{0:T(128)S(1)} %iota_convert_fusion), kind=kOutput, calls=%fused_computation.3 | convolution fusion | flops 4299161600 | bytes 14778624 | tf_op jit(solution)/shard_map/dot_general | solution.py:94
  (38 shorter events, 0.6 us)
Async XLA Ops:
  0.0 164.5 %copy-start = (bf16[1,512,2048]{2,1,0:T(8,128)(2,1)S(1)}, bf16[1,512,2048]{2,1,0:T(8,128)(2,1)}, u32[]{:S(2)}) copy-start(bf16[1,512,2048]{2,1,0:T(8,128)(2,1)} %param.25) | copy-start | bytes 6291460
  0.0 7.0 %copy-start.3 = (s32[2048]{0:T(1024)S(1)}, s32[2048]{0:T(1024)}, u32[]{:S(2)}) copy-start(s32[2048]{0:T(1024)} %param.18) | copy-start | bytes 24580
  1.9 10.7 %collective-permute-start = (f32[2,384]{0,1:T(8,128)S(1)}, f32[2,384]{0,1:T(8,128)S(1)}, u32[]{:S(2)}, u32[]{:S(2)}) collective-permute-start(f32[2,384]{0,1:T(8,128)S(1)} %copy.19), channel_id=1, source_target_pairs={{0,4},{4,8},{8,12},{12,16},{16,20},{20,24},{24,28},{28,32},{32,36}... | collective-permute-start | bytes 9224 | tf_op jit(solution)/shard_map/ppermute | solution.py:16
  7.0 3.5 %copy-start.5 = (bf16[3,256]{1,0:T(4,128)(2,1)S(1)}, bf16[3,256]{1,0:T(4,128)(2,1)}, u32[]{:S(2)}) copy-start(bf16[3,256]{1,0:T(4,128)(2,1)} %param.17) | copy-start | bytes 4612
  10.4 2.2 copy-start.4
  17.1 6.1 %copy-start.6 = (s32[512,2]{0,1:T(2,128)S(1)}, s32[512,2]{0,1:T(2,128)}, u32[]{:S(2)}) copy-start(s32[512,2]{0,1:T(2,128)} %param.21) | copy-start | bytes 12292
  18.2 20.8 %all-to-all-start = ((bf16[4,512,256]{1,2,0:T(8,128)(2,1)}), bf16[4,512,256]{1,2,0:T(8,128)(2,1)S(1)}, u32[]{:S(2)}, u32[]{:S(2)}) async-start(bf16[4,512,256]{1,2,0:T(8,128)(2,1)} %pad_maximum_fusion.1), calls=%async_computation | async-start | bytes 2097152 | tf_op jit(solution)/shard_map/all_to_all | solution.py:54
  39.0 5.8 %copy-start.2 = (pred[2048,512]{1,0:T(32,128)(4,1)S(1)}, pred[2048,512]{1,0:T(32,128)(4,1)}, u32[]{:S(2)}) copy-start(pred[2048,512]{1,0:T(32,128)(4,1)} %bitcast_compare_fusion) | copy-start | bytes 3145732
  39.0 5.8 %copy-start.10 = (f32[2048]{0:T(1024)S(1)}, f32[2048]{0:T(1024)}, u32[]{:S(2)}) copy-start(f32[2048]{0:T(1024)} %param.20) | copy-start | bytes 24580
  44.8 5.1 %copy-start.1 = (f32[512,2048]{1,0:T(8,128)}, f32[512,2048]{1,0:T(8,128)S(1)}, u32[]{:S(2)}) copy-start(f32[512,2048]{1,0:T(8,128)S(1)} %get-tuple-element.19) | copy-start | bytes 12582916
  49.9 104.8 %copy-start.8 = (bf16[1,2048,512]{2,1,0:T(8,128)(2,1)S(1)}, bf16[1,2048,512]{2,1,0:T(8,128)(2,1)}, u32[]{:S(2)}) copy-start(bf16[1,2048,512]{2,1,0:T(8,128)(2,1)} %param.23) | copy-start | bytes 6291460
  154.7 4.5 %copy-start.9 = (bf16[1,2048,512]{2,1,0:T(8,128)(2,1)S(1)}, bf16[1,2048,512]{2,1,0:T(8,128)(2,1)}, u32[]{:S(2)}) copy-start(bf16[1,2048,512]{2,1,0:T(8,128)(2,1)} %param.24) | copy-start | bytes 6291460
  171.2 5.1 %copy-start.7 = (f32[512,2]{0,1:T(2,128)S(1)}, f32[512,2]{0,1:T(2,128)}, u32[]{:S(2)}) copy-start(f32[512,2]{0,1:T(2,128)} %param.22) | copy-start | bytes 12292
  171.2 111.0 %all-to-all-start.2 = ((bf16[32,64,2048]{2,1,0:T(8,128)(2,1)}), bf16[32,64,2048]{2,1,0:T(8,128)(2,1)}, u32[]{:S(2)}, u32[]{:S(2)}) async-start(bf16[32,64,2048]{2,1,0:T(8,128)(2,1)} %bitcast.47), calls=%async_computation.2 | async-start | bytes 16777216 | tf_op jit(solution)/shard_map/all_to_all | solution.py:91
